TPU v7x, 32 devices: a whole 2x2x4 slice. The times are simulated.
32 devices in a mesh: sp: 8 (over z, x), tp: 4 (over y, core).
Axes of the slice: x: 2, y: 2, z: 4, core: 2. Of those that a mesh axis runs over, the one named last changes fastest.
Arguments:
- queries: bfloat16 [2048, 2048], P('sp', 'tp'), may hold values from -100 to 100
- key_columns: bfloat16 [1024, 2048], P('tp', 'sp'), may hold values from -24 to 24
- value_columns: bfloat16 [1024, 2048], P('tp', 'sp'), may hold values from -24 to 24
- sink_logits: float32 [32], P('tp'), may hold values from 3 to 7
- out_weight: bfloat16 [2048, 2048], P('tp'), may hold values from -0.1875 to 0.1875
- stream_in: bfloat16 [2048, 2048], P('sp'), may hold values from -3 to 3
- norm_gain: float32 [2048], replicated, may hold values from 0.1 to 1.9
- expert_ids: int32 [2048, 2], P('sp'), may hold values from 0 to 7, all different within a row; in each aligned block of 256 rows (0 to 255, 256 to 511, ...) at most 128 rows name the same one
- route_weights: float32 [2048, 2], P('sp'), may hold values from 0.1 to 0.7
- gate_weight: bfloat16 [8, 2048, 4096], P('sp', None, 'tp'), may hold values from -0.125 to 0.125
- up_weight: bfloat16 [8, 2048, 4096], P('sp', None, 'tp'), may hold values from -0.125 to 0.125
- down_weight: bfloat16 [8, 4096, 2048], P('sp', 'tp'), may hold values from -0.125 to 0.125
Outputs:
- layer_out: bfloat16 [2048, 2048], P('sp', 'tp')
Inputs may be any that keep to these rules, and one draw needn't show every extreme that they name: `expert_ids`: each row names 2 different experts. In each aligned block of 256 tokens no expert is named by more than 128 rows, and in some blocks one expert is named by exactly 128 rows.
All inputs are finite; a program needn't handle non-finite values.
Results may differ from a plain program's by a relative error of at most 0.02.
Values may be sent and summed in bfloat16 or wider, within the bound.
A program may use at most 64 MiB of HBM per device.

v0:
```python
import functools
import math

import jax
import jax.numpy as jnp
from jax import lax
from jax.experimental import pallas as pl
from jax.experimental.pallas import tpu as pltpu
from jax.sharding import PartitionSpec as P

HD = 64
WINDOW = 128
CORES = 2
EPSILON = 1e-06
MASKED = -1e30
MESH = pl.DeviceIdType.MESH
F32 = jnp.float32
BF16 = jnp.bfloat16


def iota(shape, dim):
    return lax.broadcasted_iota(jnp.int32, shape, dim)


def dot(a, b):
    return jnp.dot(a, b, preferred_element_type=F32)


def as_row(column):
    size = column.shape[0]
    eye = iota((size, size), 0) == iota((size, size), 1)
    return jnp.sum(jnp.where(eye, column, 0.0), axis=0, keepdims=True)


def as_column(row):
    size = row.shape[1]
    eye = iota((size, size), 0) == iota((size, size), 1)
    return jnp.sum(jnp.where(eye, row, 0.0), axis=1, keepdims=True)


def send(src, dst, send_sem, recv_sem, device):
    copy = pltpu.make_async_remote_copy(
        src_ref=src,
        dst_ref=dst,
        send_sem=send_sem,
        recv_sem=recv_sem,
        device_id=device,
        device_id_type=MESH,
    )
    copy.start()


def sent(ref, sem, device):
    pltpu.make_async_remote_copy(
        src_ref=ref, dst_ref=ref, send_sem=sem, recv_sem=sem,
        device_id=device, device_id_type=MESH,
    ).wait_send()


def landed(ref, sem, device):
    pltpu.make_async_remote_copy(
        src_ref=ref, dst_ref=ref, send_sem=sem, recv_sem=sem,
        device_id=device, device_id_type=MESH,
    ).wait_recv()


def layer(
    n, tp, cap,
    q_ref, k_ref, v_ref, sink_ref, gain_ref, ids_ref, rw_ref,
    ow_hbm, stream_hbm, gate_hbm, up_hbm, down_hbm,
    out_ref,
    ow, stream, gate, up, down,
    halo, head, part, part_in, part_sum, part_y, squares,
    slots, xb, hid, po, po_in, chip_sum, sum_y, final, back, residual,
    load_sem, halo_send, halo_recv, ps_send, ps_recv, py_send, py_recv, sq_send, sq_recv,
    d_send, x_recv, fc_send, fy_send, f2_send,
    po_send, po_recv, y_send, y_recv, r_send, r_recv,
):
    s, t = lax.axis_index("sp"), lax.axis_index("tp")
    ny = tp // CORES
    y, c = t // CORES, lax.rem(t, CORES)
    other = 1 - c
    tok, width = residual.shape
    hidden = gate.shape[1]

    def at_sp(i):
        return (i, t)

    def at_tp(j):
        return (s, j)

    partner = at_tp(y * CORES + other)

    def pair(i):
        total, bit = 0, 1
        while bit < n:
            total = total + lax.rem(s // bit + i // bit, 2) * bit
            bit *= 2
        return total

    def peer_y(dy):
        return lax.rem(y + dy, ny)

    def from_y(dy):
        return lax.rem(y + ny - dy, ny)

    loads = [
        pltpu.make_async_copy(ow_hbm, ow, load_sem.at[0]),
        pltpu.make_async_copy(
            stream_hbm.at[:, pl.ds(pl.multiple_of(t * width, 128), width)], stream, load_sem.at[1]
        ),
        pltpu.make_async_copy(gate_hbm.at[0], gate, load_sem.at[2]),
        pltpu.make_async_copy(up_hbm.at[0], up, load_sem.at[3]),
        pltpu.make_async_copy(down_hbm.at[0], down, load_sem.at[4]),
    ]
    for load in loads:
        load.start()

    barrier = pltpu.get_barrier_semaphore()

    def greet_sp(i, _):
        pl.semaphore_signal(
            barrier, inc=1, device_id=at_sp(lax.rem(s + i, n)), device_id_type=MESH
        )
        return 0

    def greet_tp(j, _):
        pl.semaphore_signal(
            barrier, inc=1, device_id=at_tp(lax.rem(t + j, tp)), device_id_type=MESH
        )
        return 0

    lax.fori_loop(1, n, greet_sp, 0)
    lax.fori_loop(1, tp, greet_tp, 0)
    pl.semaphore_wait(barrier, n - 1 + tp - 1)

    right, left = at_sp(lax.rem(s + 1, n)), at_sp(lax.rem(s + n - 1, n))
    for a, source in enumerate((k_ref, v_ref)):
        send(source.at[:, pl.ds(tok - WINDOW, WINDOW)], halo.at[a, 0],
             halo_send.at[a, 0], halo_recv.at[a, 0], right)
        send(source.at[:, pl.ds(0, WINDOW)], halo.at[a, 1],
             halo_send.at[a, 1], halo_recv.at[a, 1], left)

    experts = n
    lanes = iota((tok, 128), 1).astype(F32)
    top = ids_ref.shape[0]
    ids = [as_column(ids_ref[k : k + 1, :].astype(F32)) for k in range(top)]
    hits = [(lanes == ids[k]).astype(F32) for k in range(top)]
    all_hits = functools.reduce(jnp.add, hits)
    before = (iota((tok, tok), 1) < iota((tok, tok), 0)).astype(BF16)
    earlier = dot(before, all_hits.astype(BF16))
    place = [
        jnp.sum(earlier * hits[k], axis=1, keepdims=True) + ids[k] * cap
        for k in range(top)
    ]
    place_row = [as_row(p) for p in place]

    for a, source in enumerate((k_ref, v_ref)):
        landed(halo.at[a, 0], halo_recv.at[a, 0], left)
        landed(halo.at[a, 1], halo_recv.at[a, 1], right)

    kv_heads = k_ref.shape[0] // HD
    group = q_ref.shape[1] // HD // kv_heads
    span = 3 * WINDOW
    row = lax.rem(iota((group * WINDOW, span), 0), WINDOW)
    col = iota((group * WINDOW, span), 1)
    near = (col - row >= 0) & (col - row <= 2 * WINDOW)
    for b in range(tok // WINDOW):
        key_pos = s * tok + (b - 1) * WINDOW + col
        visible = near & (key_pos >= 0) & (key_pos < n * tok)
        rows = pl.ds(b * WINDOW, WINDOW)
        for g in range(kv_heads):
            feats = pl.ds(g * HD, HD)
            kx, vx = [
                jnp.concatenate(
                    [halo[a, 0, feats, :], ref[feats, :], halo[a, 1, feats, :]], axis=1
                )[:, b * WINDOW : b * WINDOW + span]
                for a, ref in enumerate((k_ref, v_ref))
            ]
            qs = jnp.concatenate(
                [q_ref[rows, pl.ds((g * group + h) * HD, HD)] for h in range(group)], axis=0
            )
            sink = jnp.concatenate(
                [jnp.full((WINDOW, 1), sink_ref[g * group + h], F32) for h in range(group)], axis=0
            )
            scores = jnp.where(visible, dot(qs, kx) * (1.0 / math.sqrt(HD)), MASKED)
            row_top = jnp.maximum(jnp.max(scores, axis=1, keepdims=True), sink)
            weight = jnp.where(visible, jnp.exp(scores - row_top), 0.0)
            total = jnp.sum(weight, axis=1, keepdims=True) + jnp.exp(sink - row_top)
            weight = (weight * (1.0 / total)).astype(BF16)
            mixed = lax.dot_general(
                weight, vx, (((1,), (1,)), ((), ())), preferred_element_type=F32
            ).astype(BF16)
            head[rows, pl.ds(g * group * HD, group * HD)] = jnp.concatenate(
                [mixed[h * WINDOW : (h + 1) * WINDOW] for h in range(group)], axis=1
            )

    loads[0].wait()
    loads[1].wait()

    def project(core):
        for yy in range(ny):
            start = pl.multiple_of((yy * CORES + core) * width, 128)
            part[core, yy] = dot(head[...], ow[:, pl.ds(start, width)]).astype(BF16)

    project(other)
    send(part.at[other], part_in, ps_send, ps_recv, partner)
    project(c)
    landed(part_in, ps_recv, partner)
    for dy in range(1, ny):
        yy = peer_y(dy)
        part_sum[dy] = (part[c, yy].astype(F32) + part_in[yy].astype(F32)).astype(BF16)
        send(part_sum.at[dy], part_y.at[dy], py_send.at[dy], py_recv.at[dy],
             at_tp(yy * CORES + c))
    attn = part[c, y].astype(F32) + part_in[y].astype(F32)
    for dy in range(1, ny):
        landed(part_y.at[dy], py_recv.at[dy], at_tp(from_y(dy) * CORES + c))
        attn = attn + part_y[dy].astype(F32)
    res = (stream[...].astype(F32) + attn.astype(BF16).astype(F32)).astype(BF16)
    residual[...] = res
    res = res.astype(F32)
    own_squares = jnp.broadcast_to(as_row(jnp.sum(res * res, axis=1, keepdims=True)), (8, tok))
    squares[0] = own_squares
    for dt in range(1, tp):
        send(squares.at[0], squares.at[dt], sq_send.at[dt], sq_recv.at[dt],
             at_tp(lax.rem(t + dt, tp)))
    square_sum = own_squares
    for dt in range(1, tp):
        landed(squares.at[dt], sq_recv.at[dt], at_tp(lax.rem(t + tp - dt, tp)))
        square_sum = square_sum + squares[dt]
    inverse = as_column(lax.rsqrt(square_sum[0:1] / (tp * width) + EPSILON))
    gain = gain_ref[:, pl.ds(pl.multiple_of(t * width, 128), width)]
    normed = (res * inverse * gain).astype(BF16)

    slot = iota((cap, tok), 0)

    def rows_of(e):
        wanted = (slot + e * cap).astype(F32)
        pick = functools.reduce(jnp.logical_or, [wanted == p for p in place_row])
        return dot(pick.astype(F32).astype(BF16), normed).astype(BF16)

    xb[t, s] = rows_of(s)

    def dispatch(i, _):
        e = pair(i)
        slots[i] = rows_of(e)
        send(slots.at[i], xb.at[t, s], d_send.at[i], x_recv.at[t, s], at_sp(e))
        return 0

    lax.fori_loop(1, n, dispatch, 0)
    for load in loads[2:]:
        load.wait()

    def forward(i):
        src = pair(i)

        @pl.when(i > 0)
        def _():
            landed(xb.at[t, src], x_recv.at[t, src], at_sp(src))

        for dy in range(1, ny):
            send(xb.at[t, src], xb.at[t, src], fy_send.at[dy, i], x_recv.at[t, src],
                 at_tp(peer_y(dy) * CORES + c))
        send(xb.at[t, src], xb.at[t, src], fc_send.at[i], x_recv.at[t, src], partner)

    def relay(i):
        src = pair(i)
        for dy in range(1, ny):
            j = from_y(dy) * CORES + c
            landed(xb.at[j, src], x_recv.at[j, src], at_tp(j))
            send(xb.at[j, src], xb.at[j, src], f2_send.at[dy, i], x_recv.at[j, src], partner)

    tile = min(hidden, 256)

    def expert(i):
        src = pair(i)
        for yy in range(ny):
            j = yy * CORES + other
            landed(xb.at[j, src], x_recv.at[j, src], partner)
        rows = jnp.concatenate([xb[j, src] for j in range(tp)], axis=1)
        for f in range(hidden // tile):
            cols = pl.ds(f * tile, tile)
            gate_pre = dot(rows, gate[:, cols])
            upward = dot(rows, up[:, cols])
            hid[:, cols] = (gate_pre / (1.0 + jnp.exp(-gate_pre)) * upward).astype(BF16)
        for j in range(tp):
            po[i, j % CORES, j // CORES] = dot(
                hid[...], down[:, j * width : (j + 1) * width]
            ).astype(BF16)
        send(po.at[i, other], po_in.at[i], po_send.at[i], po_recv.at[i], partner)

    def chip_add(i):
        landed(po_in.at[i], po_recv.at[i], partner)
        for dy in range(1, ny):
            yy = peer_y(dy)
            chip_sum[dy, i] = (po[i, c, yy].astype(F32) + po_in[i, yy].astype(F32)).astype(BF16)
            send(chip_sum.at[dy, i], sum_y.at[dy, i], y_send.at[dy, i], y_recv.at[dy, i],
                 at_tp(yy * CORES + c))

    def finish(i):
        src = pair(i)
        total = po[i, c, y].astype(F32) + po_in[i, y].astype(F32)
        for dy in range(1, ny):
            landed(sum_y.at[dy, i], y_recv.at[dy, i], at_tp(from_y(dy) * CORES + c))
            total = total + sum_y[dy, i].astype(F32)

        @pl.when(i == 0)
        def _():
            back[s] = total.astype(BF16)

        @pl.when(i > 0)
        def _():
            final[i] = total.astype(BF16)
            send(final.at[i], back.at[s], r_send.at[i], r_recv.at[s], at_sp(src))

    stages = (forward, relay, expert, chip_add, finish)

    def step(k, _):
        for lag, stage in reversed(tuple(enumerate(stages))):
            @pl.when((k >= lag) & (k - lag < n))
            def _(stage=stage, lag=lag):
                stage(k - lag)
        return 0

    lax.fori_loop(0, n + len(stages) - 1, step, 0)

    def returned(i, _):
        e = lax.rem(s + i, n)
        landed(back.at[e], r_recv.at[e], at_sp(e))
        return 0

    lax.fori_loop(1, n, returned, 0)

    rows = back[...].reshape(n * cap, width)
    spot = iota((tok, n * cap), 1).astype(F32)
    mixture = jnp.zeros((tok, width), F32)
    for k in range(top):
        pick = (spot == place[k]).astype(F32).astype(BF16)
        mixture = mixture + as_column(rw_ref[k : k + 1, :]) * dot(pick, rows)
    out_ref[...] = (residual[...].astype(F32) + mixture).astype(BF16)

    for a, source in enumerate((k_ref, v_ref)):
        sent(halo.at[a, 0], halo_send.at[a, 0], right)
        sent(halo.at[a, 1], halo_send.at[a, 1], left)
    sent(part.at[other], ps_send, partner)
    for dy in range(1, ny):
        sent(part_sum.at[dy], py_send.at[dy], partner)
    for dt in range(1, tp):
        sent(squares.at[0], sq_send.at[dt], partner)

    def drain(i, _):
        @pl.when(i > 0)
        def _():
            sent(slots.at[i], d_send.at[i], right)
            sent(final.at[i], r_send.at[i], right)

        sent(final.at[i], fc_send.at[i], partner)
        sent(po_in.at[i], po_send.at[i], partner)
        for dy in range(1, ny):
            sent(final.at[i], fy_send.at[dy, i], partner)
            sent(final.at[i], f2_send.at[dy, i], partner)
            sent(final.at[i], y_send.at[dy, i], partner)
        return 0

    lax.fori_loop(0, n, drain, 0)


def local(
    n, tp,
    queries, key_columns, value_columns, sink_logits, out_weight, stream_in, norm_gain,
    expert_ids, route_weights, gate_weight, up_weight, down_weight,
):
    tok, features = stream_in.shape
    ny = tp // CORES
    cap = 4 * tok // n
    width = features // tp
    hidden = gate_weight.shape[2]
    kv = key_columns.shape[0]
    dma = pltpu.SemaphoreType.DMA
    vmem = pl.BlockSpec(memory_space=pltpu.VMEM)
    hbm = pl.BlockSpec(memory_space=pl.ANY)
    smem = pl.BlockSpec(memory_space=pltpu.SMEM)
    scratch = [
        pltpu.VMEM(out_weight.shape, BF16),
        pltpu.VMEM((tok, width), BF16),
        pltpu.VMEM(gate_weight.shape[1:], BF16),
        pltpu.VMEM(up_weight.shape[1:], BF16),
        pltpu.VMEM(down_weight.shape[1:], BF16),
        pltpu.VMEM((2, 2, kv, WINDOW), BF16),
        pltpu.VMEM(queries.shape, BF16),
        pltpu.VMEM((CORES, ny, tok, width), BF16),
        pltpu.VMEM((ny, tok, width), BF16),
        pltpu.VMEM((ny, tok, width), BF16),
        pltpu.VMEM((ny, tok, width), BF16),
        pltpu.VMEM((tp, 8, tok), F32),
        pltpu.VMEM((n, cap, width), BF16),
        pltpu.VMEM((tp, n, cap, width), BF16),
        pltpu.VMEM((cap, hidden), BF16),
        pltpu.VMEM((n, CORES, ny, cap, width), BF16),
        pltpu.VMEM((n, ny, cap, width), BF16),
        pltpu.VMEM((ny, n, cap, width), BF16),
        pltpu.VMEM((ny, n, cap, width), BF16),
        pltpu.VMEM((n, cap, width), BF16),
        pltpu.VMEM((n, cap, width), BF16),
        pltpu.VMEM((tok, width), BF16),
        dma((5,)),
        dma((2, 2)), dma((2, 2)),
        dma, dma,
        dma((ny,)), dma((ny,)),
        dma((tp,)), dma((tp,)),
        dma((n,)), dma((tp, n)), dma((n,)), dma((ny, n)), dma((ny, n)),
        dma((n,)), dma((n,)),
        dma((ny, n)), dma((ny, n)),
        dma((n,)), dma((n,)),
    ]
    return pl.pallas_call(
        functools.partial(layer, n, tp, cap),
        out_shape=jax.ShapeDtypeStruct((tok, width), BF16),
        in_specs=[vmem, vmem, vmem, smem, vmem, vmem, vmem] + [hbm] * 5,
        out_specs=vmem,
        scratch_shapes=scratch,
        compiler_params=pltpu.CompilerParams(
            collective_id=0, has_side_effects=True, vmem_limit_bytes=60 * 1024 * 1024
        ),
    )(
        queries, key_columns, value_columns, sink_logits, norm_gain[None, :], expert_ids.T,
        route_weights.T, out_weight, stream_in, gate_weight, up_weight, down_weight,
    )


def solution(mesh):
    placed = (
        P("sp", "tp"),
        P("tp", "sp"),
        P("tp", "sp"),
        P("tp"),
        P("tp", None),
        P("sp", None),
        P(),
        P("sp", None),
        P("sp", None),
        P("sp", None, "tp"),
        P("sp", None, "tp"),
        P("sp", "tp", None),
    )
    return jax.shard_map(
        functools.partial(local, mesh.shape["sp"], mesh.shape["tp"]),
        mesh=mesh, in_specs=placed, out_specs=P("sp", "tp"), check_vma=False,
    )
```

profile of v0, /device:TPU:8, one launch (start us, length us, event | category | flops | bytes accessed | tf_op | source)
XLA Modules:
  0.0 98.7 jit_solution(3294008590851838673)
XLA Ops:
  0.0 97.1 %shard_map.118 = bf16[256,512]{1,0:T(8,128)(2,1)} custom-call(bf16[256,512]{1,0:T(8,128)(2,1)} %q_ref.1, bf16[256,256]{1,0:T(8,128)(2,1)} %k_ref.1, bf16[256,256]{1,0:T(8,128)(2,1)} %v_ref.1, f32[8]{0:T(128)} %sink_ref.1, f32[1,2048]{1,0:T(1,128)} %bitcast.3, s32[2,256]{1,0:T(2,128)} %bitcast.4, f32[2,256]{1,0:T(2,128)} %bitcast.5, ...), custom_call_target="tpu_custom_call" | custom-call | tf_op jit(solution)/shard_map/pallas_call | solution.py:416
  97.1 1.7 %copy.14 = bf16[256,512]{1,0:T(8,128)(2,1)} copy(bf16[256,512]{1,0:T(8,128)(2,1)} %shard_map.118) | data formatting | bytes 524288
where the time goes:
time: 98.9 us; the launch traced here: 98.7 us
  Pallas kernels  97.1 us (98%)
  local copies, waits for them, and re-layouts  1.67 us (2%)
    pallas_call x1, Pallas kernels, local(): pl.pallas_call(functools.partial(layer, n, tp, cap), out_shape=jax.ShapeD...  97.1 us

commit v1 on v0

v1 whole, which is shorter than its diff:
```python
import functools
import math

import jax
import jax.numpy as jnp
from jax import lax
from jax.experimental import pallas as pl
from jax.experimental.pallas import tpu as pltpu
from jax.sharding import PartitionSpec as P

HD = 64
WINDOW = 128
CORES = 2
BLOCKS = 2
EPSILON = 1e-06
MASKED = -1e30
MESH = pl.DeviceIdType.MESH
F32 = jnp.float32
BF16 = jnp.bfloat16
scope = jax.named_scope


def iota(shape, dim):
    return lax.broadcasted_iota(jnp.int32, shape, dim)


def dot(a, b):
    return jnp.dot(a, b, preferred_element_type=F32)


def dot_t(a, b):
    return lax.dot_general(a, b, (((1,), (1,)), ((), ())), preferred_element_type=F32)


def as_row(column):
    size = column.shape[0]
    eye = iota((size, size), 0) == iota((size, size), 1)
    return jnp.sum(jnp.where(eye, column, 0.0), axis=0, keepdims=True)


def as_column(row):
    size = row.shape[1]
    eye = iota((size, size), 0) == iota((size, size), 1)
    return jnp.sum(jnp.where(eye, row, 0.0), axis=1, keepdims=True)


def diagonal(a):
    zero = jnp.zeros(a.shape, a.dtype)
    return jnp.concatenate(
        [jnp.concatenate([a, zero], axis=1), jnp.concatenate([zero, a], axis=1)], axis=0
    )


def send(src, dst, send_sem, recv_sem, device):
    pltpu.make_async_remote_copy(
        src_ref=src,
        dst_ref=dst,
        send_sem=send_sem,
        recv_sem=recv_sem,
        device_id=device,
        device_id_type=MESH,
    ).start()


def sent(ref, sem, device):
    pltpu.make_async_remote_copy(
        src_ref=ref, dst_ref=ref, send_sem=sem, recv_sem=sem,
        device_id=device, device_id_type=MESH,
    ).wait_send()


def landed(ref, sem, device):
    pltpu.make_async_remote_copy(
        src_ref=ref, dst_ref=ref, send_sem=sem, recv_sem=sem,
        device_id=device, device_id_type=MESH,
    ).wait_recv()


def layer(
    n, tp, cap,
    q_hbm, k_hbm, v_hbm, sink_hbm, gain_hbm, ids_hbm, rw_hbm,
    ow_hbm, stream_hbm, gate_hbm, up_hbm, down_hbm,
    out_hbm,
    q_ref, k_ref, v_ref, sink_ref, gain_ref, ids_ref, rw_ref,
    ow, stream, gate, up, down,
    halo, own_o, own_m, head, part, part_in, part_sum, part_y, squares,
    pick, mixer, rows_out, slots, scale_out, scale_in, xb, hid,
    po, po_in, chip_sum, sum_y, final, back, mixed, residual, out,
    load_sem, halo_send, halo_recv, ps_send, ps_recv, py_send, py_recv, sq_send, sq_recv,
    d_send, x_recv, sc_send, sc_recv, fc_send, fy_send, f2_send,
    po_send, po_recv, y_send, y_recv, r_send, r_recv, out_sem,
):
    s, t = lax.axis_index("sp"), lax.axis_index("tp")
    ny = tp // CORES
    y, c = t // CORES, lax.rem(t, CORES)
    other = 1 - c
    tok, width = residual.shape
    hidden = gate.shape[1]
    top = ids_ref.shape[0]
    kv_heads = k_ref.shape[0] // HD

    def at_sp(i):
        return (i, t)

    def at_tp(j):
        return (s, j)

    partner = at_tp(y * CORES + other)

    def pair(i):
        total, bit = 0, 1
        while bit < n:
            total = total + lax.rem(s // bit + i // bit, 2) * bit
            bit *= 2
        return total

    def peer_y(dy):
        return lax.rem(y + dy, ny)

    def from_y(dy):
        return lax.rem(y + ny - dy, ny)

    own_cols = pl.ds(pl.multiple_of(t * width, 128), width)
    loads = [
        pltpu.make_async_copy(src, dst, load_sem.at[i])
        for i, (src, dst) in enumerate((
            (k_hbm, k_ref), (v_hbm, v_ref), (q_hbm, q_ref), (ids_hbm, ids_ref),
            (sink_hbm, sink_ref), (rw_hbm, rw_ref), (gain_hbm, gain_ref),
            (ow_hbm, ow), (stream_hbm.at[:, own_cols], stream),
            (gate_hbm.at[0], gate), (up_hbm.at[0], up), (down_hbm.at[0], down),
        ))
    ]
    for load in loads[:7]:
        load.start()

    barrier = pltpu.get_barrier_semaphore()

    def greet_sp(i, _):
        pl.semaphore_signal(
            barrier, inc=1, device_id=at_sp(lax.rem(s + i, n)), device_id_type=MESH
        )
        return 0

    def greet_tp(j, _):
        pl.semaphore_signal(
            barrier, inc=1, device_id=at_tp(lax.rem(t + j, tp)), device_id_type=MESH
        )
        return 0

    lax.fori_loop(1, n, greet_sp, 0)
    lax.fori_loop(1, tp, greet_tp, 0)
    loads[0].wait()
    loads[1].wait()
    loads[3].wait()
    for load in loads[7:9]:
        load.start()
    with scope("barrier"):
        pl.semaphore_wait(barrier, n - 1 + tp - 1)

    right, left = at_sp(lax.rem(s + 1, n)), at_sp(lax.rem(s + n - 1, n))
    last = tok - WINDOW

    def send_right():
        @pl.when(s < n - 1)
        def _():
            for a, source in enumerate((k_ref, v_ref)):
                send(source.at[:, pl.ds(last, WINDOW)], halo.at[a, 0],
                     halo_send.at[a, 0], halo_recv.at[a, 0], right)

    def send_left():
        @pl.when(s > 0)
        def _():
            for a, source in enumerate((k_ref, v_ref)):
                send(source.at[:, pl.ds(0, WINDOW)], halo.at[a, 1],
                     halo_send.at[a, 1], halo_recv.at[a, 1], left)

    even = lax.rem(s, 2) == 0
    pl.when(even)(send_right)
    send_left()
    pl.when(jnp.logical_not(even))(send_right)
    for load in loads[9:]:
        load.start()

    @pl.when(s == 0)
    def _():
        for a in range(2):
            halo[a, 0] = jnp.zeros(halo.shape[2:], BF16)

    @pl.when(s == n - 1)
    def _():
        for a in range(2):
            halo[a, 1] = jnp.zeros(halo.shape[2:], BF16)

    loads[2].wait()
    loads[4].wait()
    square = (WINDOW, WINDOW)
    ahead = iota(square, 1) - iota(square, 0)
    low_lanes = iota(square, 1) < HD

    def query(b, g):
        rows = pl.ds(pl.multiple_of(b * WINDOW, WINDOW), WINDOW)
        return q_ref[rows, pl.ds(g * 2 * HD, 2 * HD)] * (1.0 / math.sqrt(HD))

    def mix_matrix(v):
        return jnp.concatenate([diagonal(v), diagonal(jnp.ones(v.shape, BF16))], axis=0)

    def sinks(g):
        return [sink_ref[0:1, 2 * g + h : 2 * g + h + 1] for h in range(2)]

    with scope("attn_own"):
        for g in range(kv_heads):
            feats = pl.ds(g * HD, HD)
            keys = diagonal(k_ref[feats, :])
            mixer_v = mix_matrix(v_ref[feats, :])
            for b in range(BLOCKS):
                scores = dot(query(b, g), keys)
                weights = []
                for h in range(2):
                    part_s = [
                        scores[:, h * tok + kb * WINDOW : h * tok + (kb + 1) * WINDOW]
                        for kb in range(BLOCKS)
                    ]
                    if b == 0:
                        part_s[1] = jnp.where(ahead <= 0, part_s[1], MASKED)
                    else:
                        part_s[0] = jnp.where(ahead >= 0, part_s[0], MASKED)
                    row_top = jnp.max(
                        jnp.maximum(part_s[0], part_s[1]), axis=1, keepdims=True
                    )
                    row_top = jnp.maximum(row_top, sinks(g)[h])
                    own_m[b, g, h] = jnp.broadcast_to(row_top, square)
                    weights += [jnp.exp(p - row_top).astype(BF16) for p in part_s]
                own_o[b, g] = dot_t(jnp.concatenate(weights, axis=1), mixer_v)

    with scope("routing"):
        lanes = iota((tok, 128), 1).astype(F32)
        ids = [as_column(ids_ref[k : k + 1, :].astype(F32)) for k in range(top)]
        hits = [(lanes == ids[k]).astype(F32) for k in range(top)]
        all_hits = functools.reduce(jnp.add, hits)
        before = (iota((tok, tok), 1) < iota((tok, tok), 0)).astype(BF16)
        earlier = dot(before, all_hits.astype(BF16))
        place = [
            jnp.sum(earlier * hits[k], axis=1, keepdims=True) + ids[k] * cap
            for k in range(top)
        ]
        place_row = [as_row(p) for p in place]
        loads[5].wait()
        share = [as_column(rw_ref[k : k + 1, :]) for k in range(top)]

        def picks(i, _):
            base = pair(i) * cap
            wanted = (iota((cap, tok), 0) + base).astype(F32)
            hit = functools.reduce(jnp.logical_or, [wanted == p for p in place_row])
            pick[pl.ds(pl.multiple_of(i * cap, cap), cap), :] = hit.astype(F32).astype(BF16)
            spot = (iota((tok, cap), 1) + base).astype(F32)
            weight = functools.reduce(
                jnp.add, [jnp.where(spot == p, w, 0.0) for p, w in zip(place, share)]
            )
            high = weight.astype(BF16)
            mixer[i] = jnp.concatenate([high, (weight - high.astype(F32)).astype(BF16)], axis=1)
            return 0

        lax.fori_loop(0, n, picks, 0)
    loads[6].wait()
    loads[7].wait()
    loads[8].wait()
    gain = gain_ref[:, own_cols]

    def attend(b):
        side = 1 - 2 * b
        edge = s + b * n
        inside = jnp.logical_and(edge > 0, edge < 2 * n - 1)

        @pl.when(inside)
        def _():
            for a in range(2):
                landed(halo.at[a, b], halo_recv.at[a, b], left)

        visible = (ahead * side >= 0) & (jnp.broadcast_to(inside.astype(jnp.int32), square) > 0)
        rows = pl.ds(pl.multiple_of(b * WINDOW, WINDOW), WINDOW)
        for g in range(kv_heads):
            feats = pl.ds(g * HD, HD)
            scores = dot(query(b, g), diagonal(halo[0, b, feats, :]))
            weights, gap, rest = [], [], []
            for h in range(2):
                piece = jnp.where(visible, scores[:, h * WINDOW : (h + 1) * WINDOW], MASKED)
                before_top = own_m[b, g, h]
                row_top = jnp.max(jnp.maximum(piece, before_top), axis=1, keepdims=True)
                weights.append(jnp.exp(piece - row_top).astype(BF16))
                gap.append(before_top - row_top)
                rest.append(jnp.broadcast_to(sinks(g)[h] - row_top, square))
            added = dot_t(
                jnp.concatenate(weights, axis=1), mix_matrix(halo[1, b, feats, :])
            )
            old = own_o[b, g]
            shrink = jnp.exp(jnp.where(low_lanes, gap[0], gap[1]))
            total = jnp.exp(jnp.where(low_lanes, rest[0], rest[1]))
            total = total + old[:, 2 * HD :] * shrink + added[:, 2 * HD :]
            value = old[:, : 2 * HD] * shrink + added[:, : 2 * HD]
            head[rows, pl.ds(g * 2 * HD, 2 * HD)] = (value / total).astype(BF16)

    def project(b, core):
        mine = head[pl.ds(pl.multiple_of(b * WINDOW, WINDOW), WINDOW), :]
        for yy in range(ny):
            start = pl.multiple_of((yy * CORES + core) * width, 128)
            part[b, core, yy] = dot(mine, ow[:, pl.ds(start, width)]).astype(BF16)

    def swap(b):
        project(b, other)
        send(part.at[b, other], part_in.at[b], ps_send.at[b], ps_recv.at[b], partner)
        project(b, c)

    def across(b):
        landed(part_in.at[b], ps_recv.at[b], partner)
        for dy in range(1, ny):
            yy = peer_y(dy)
            part_sum[b, dy] = (
                part[b, c, yy].astype(F32) + part_in[b, yy].astype(F32)
            ).astype(BF16)
            send(part_sum.at[b, dy], part_y.at[b, dy], py_send.at[b, dy], py_recv.at[b, dy],
                 at_tp(yy * CORES + c))

    def settle(b):
        attn = part[b, c, y].astype(F32) + part_in[b, y].astype(F32)
        for dy in range(1, ny):
            landed(part_y.at[b, dy], py_recv.at[b, dy], at_tp(from_y(dy) * CORES + c))
            attn = attn + part_y[b, dy].astype(F32)
        rows = pl.ds(pl.multiple_of(b * WINDOW, WINDOW), WINDOW)
        res = (stream[rows, :].astype(F32) + attn.astype(BF16).astype(F32)).astype(BF16)
        residual[rows, :] = res
        res = res.astype(F32)
        rows_out[rows, :] = (res * gain).astype(BF16)
        squares[0, :, rows] = jnp.broadcast_to(
            as_row(jnp.sum(res * res, axis=1, keepdims=True)), (8, WINDOW)
        )

    first = 1 - lax.rem(s, 2)
    second = 1 - first
    with scope("attend0"):
        attend(first)
    with scope("swap0"):
        swap(first)
    with scope("attend1"):
        attend(second)
    with scope("across0"):
        across(first)
    with scope("swap1"):
        swap(second)
    with scope("across1"):
        across(second)
    with scope("settle0"):
        settle(first)
    with scope("settle1"):
        settle(second)
    for dt in range(1, tp):
        send(squares.at[0], squares.at[dt], sq_send.at[dt], sq_recv.at[dt],
             at_tp(lax.rem(t + dt, tp)))

    def lane(k):
        return jnp.where(k < 2, k, jnp.where(k < 2 + n // 2, k - 2 + n // 2, k - n // 2))

    def rows_of(i):
        chosen = pick[pl.ds(pl.multiple_of(i * cap, cap), cap), :]
        return dot(chosen, rows_out[...]).astype(BF16)

    def forward(k):
        i = lane(k)

        @pl.when(i > 0)
        def _():
            landed(xb.at[t, i], x_recv.at[t, i], right)

        for dy in range(1, ny):
            send(xb.at[t, i], xb.at[t, i], fy_send.at[dy, i], x_recv.at[t, i],
                 at_tp(peer_y(dy) * CORES + c))
        send(xb.at[t, i], xb.at[t, i], fc_send.at[i], x_recv.at[t, i], partner)

    def dispatch(k, _):
        i = lane(k)
        slots[i] = rows_of(i)
        send(slots.at[i], xb.at[t, i], d_send.at[i], x_recv.at[t, i], at_sp(pair(i)))
        return 0

    with scope("dispatch"):
        xb[t, 0] = rows_of(0)
        forward(0)
        lax.fori_loop(1, n, dispatch, 0)

    with scope("scales"):
        square_sum = squares[0]
        for dt in range(1, tp):
            landed(squares.at[dt], sq_recv.at[dt], at_tp(lax.rem(t + tp - dt, tp)))
            square_sum = square_sum + squares[dt]
        inverse = lax.rsqrt(square_sum / (tp * width) + EPSILON)
        high = inverse.astype(BF16).astype(F32)
        middle = (inverse - high).astype(BF16).astype(F32)
        low = inverse - high - middle
        level = iota(inverse.shape, 0)
        pieces = jnp.where(
            level == 0, high, jnp.where(level == 1, middle, jnp.where(level == 2, low, 0.0))
        ).astype(BF16)
        scales = jnp.sum(dot_t(pieces, pick[...]), axis=0, keepdims=True)
        for i in range(n):
            piece = jnp.broadcast_to(scales[:, i * cap : (i + 1) * cap], (8, cap))
            if i == 0:
                scale_in[0] = piece
            else:
                scale_out[i] = piece
                send(scale_out.at[i], scale_in.at[i], sc_send.at[i], sc_recv.at[i],
                     at_sp(pair(i)))

    with scope("weights"):
        for load in loads[9:]:
            load.wait()

    def turn(j):
        return jnp.where(
            j < n // 2, j + n // 2, jnp.where(j < n - 2, j + 2 - n // 2, n - 1 - j)
        )

    def relay(k):
        i = lane(k)
        for dy in range(1, ny):
            j = from_y(dy) * CORES + c
            landed(xb.at[j, i], x_recv.at[j, i], at_tp(j))
            send(xb.at[j, i], xb.at[j, i], f2_send.at[dy, i], x_recv.at[j, i], partner)

    tile = min(hidden, 256)

    def expert(k):
        i = turn(k)
        for yy in range(ny):
            j = yy * CORES + other
            landed(xb.at[j, i], x_recv.at[j, i], partner)

        @pl.when(i > 0)
        def _():
            landed(scale_in.at[i], sc_recv.at[i], right)

        scale = as_column(scale_in[i, 0:1, :])
        rows = jnp.concatenate([xb[j, i] for j in range(tp)], axis=1)
        for f in range(hidden // tile):
            cols = pl.ds(f * tile, tile)
            gate_pre = dot(rows, gate[:, cols]) * scale
            upward = dot(rows, up[:, cols]) * scale
            hid[:, cols] = (gate_pre / (1.0 + jnp.exp(-gate_pre)) * upward).astype(BF16)
        for j in range(tp):
            po[i, j % CORES, j // CORES] = dot(
                hid[...], down[:, j * width : (j + 1) * width]
            ).astype(BF16)
        send(po.at[i, other], po_in.at[i], po_send.at[i], po_recv.at[i], partner)

    def chip_add(k):
        i = turn(k)
        landed(po_in.at[i], po_recv.at[i], partner)
        for dy in range(1, ny):
            yy = peer_y(dy)
            chip_sum[dy, i] = (po[i, c, yy].astype(F32) + po_in[i, yy].astype(F32)).astype(BF16)
            send(chip_sum.at[dy, i], sum_y.at[dy, i], y_send.at[dy, i], y_recv.at[dy, i],
                 at_tp(yy * CORES + c))

    def whole(i):
        total = po[i, c, y].astype(F32) + po_in[i, y].astype(F32)
        for dy in range(1, ny):
            landed(sum_y.at[dy, i], y_recv.at[dy, i], at_tp(from_y(dy) * CORES + c))
            total = total + sum_y[dy, i].astype(F32)
        return total.astype(BF16)

    def finish(k):
        i = turn(k)
        final[i] = whole(i)
        send(final.at[i], back.at[i], r_send.at[i], r_recv.at[i], at_sp(pair(i)))

    stages = (
        (0, n, forward), (5, n, chip_add), (1, n, relay), (4, n, expert), (6, n - 1, finish),
    )

    def step(k, _):
        for lag, count, stage in stages:
            first_step = max(lag, 1)

            @pl.when((k >= first_step) & (k - lag < count))
            def _(stage=stage, lag=lag):
                with scope(stage.__name__):
                    stage(k - lag)
        return 0

    lax.fori_loop(1, n + 5, step, 0)

    def blend(i):
        rows = back[i]
        return dot(mixer[i], jnp.concatenate([rows, rows], axis=0))

    def returned(i, _):
        landed(back.at[i], r_recv.at[i], right)
        mixed[...] += blend(i)
        return 0

    with scope("returned"):
        mixed[...] = residual[...].astype(F32)
        lax.fori_loop(2, n, returned, 0)

    with scope("drain"):
        @pl.when(s < n - 1)
        def _():
            for a in range(2):
                sent(halo.at[a, 0], halo_send.at[a, 0], right)

        @pl.when(s > 0)
        def _():
            for a in range(2):
                sent(halo.at[a, 1], halo_send.at[a, 1], left)

        for b in range(BLOCKS):
            sent(part_in.at[b], ps_send.at[b], partner)
            for dy in range(1, ny):
                sent(part_sum.at[b, dy], py_send.at[b, dy], partner)
        for dt in range(1, tp):
            sent(squares.at[0], sq_send.at[dt], partner)

        def drain(i, _):
            @pl.when(i > 0)
            def _():
                sent(slots.at[i], d_send.at[i], right)
                sent(scale_out.at[i], sc_send.at[i], right)

            @pl.when(i > 1)
            def _():
                sent(final.at[i], r_send.at[i], right)

            sent(final.at[i], fc_send.at[i], partner)
            sent(po_in.at[i], po_send.at[i], partner)
            for dy in range(1, ny):
                sent(final.at[i], fy_send.at[dy, i], partner)
                sent(final.at[i], f2_send.at[dy, i], partner)
            return 0

        lax.fori_loop(0, n, drain, 0)

    with scope("own"):
        back[0] = whole(0)
        mixed[...] += blend(0)

    with scope("near"):
        landed(back.at[1], r_recv.at[1], right)
        out[...] = (mixed[...] + blend(1)).astype(BF16)
    put = pltpu.make_async_copy(out, out_hbm, out_sem)
    put.start()
    sent(final.at[1], r_send.at[1], right)

    def drain_y(i, _):
        for dy in range(1, ny):
            sent(final.at[i], y_send.at[dy, i], partner)
        return 0

    with scope("exit"):
        lax.fori_loop(0, n, drain_y, 0)
        put.wait()


def local(
    n, tp,
    queries, key_columns, value_columns, sink_logits, out_weight, stream_in, norm_gain,
    expert_ids, route_weights, gate_weight, up_weight, down_weight,
):
    tok, features = stream_in.shape
    ny = tp // CORES
    cap = 4 * tok // n
    width = features // tp
    hidden = gate_weight.shape[2]
    kv = key_columns.shape[0]
    top = expert_ids.shape[1]
    heads = sink_logits.shape[0]
    groups = kv // HD
    assert tok == BLOCKS * WINDOW and heads == 2 * groups
    dma = pltpu.SemaphoreType.DMA
    anywhere = pl.BlockSpec(memory_space=pl.ANY)
    scratch = [
        pltpu.VMEM(queries.shape, BF16),
        pltpu.VMEM(key_columns.shape, BF16),
        pltpu.VMEM(value_columns.shape, BF16),
        pltpu.VMEM((1, heads), F32),
        pltpu.VMEM((1, features), F32),
        pltpu.VMEM((top, tok), jnp.int32),
        pltpu.VMEM((top, tok), F32),
        pltpu.VMEM(out_weight.shape, BF16),
        pltpu.VMEM((tok, width), BF16),
        pltpu.VMEM(gate_weight.shape[1:], BF16),
        pltpu.VMEM(up_weight.shape[1:], BF16),
        pltpu.VMEM(down_weight.shape[1:], BF16),
        pltpu.VMEM((2, 2, kv, WINDOW), BF16),
        pltpu.VMEM((BLOCKS, groups, WINDOW, 4 * HD), F32),
        pltpu.VMEM((BLOCKS, groups, 2, WINDOW, WINDOW), F32),
        pltpu.VMEM(queries.shape, BF16),
        pltpu.VMEM((BLOCKS, CORES, ny, WINDOW, width), BF16),
        pltpu.VMEM((BLOCKS, ny, WINDOW, width), BF16),
        pltpu.VMEM((BLOCKS, ny, WINDOW, width), BF16),
        pltpu.VMEM((BLOCKS, ny, WINDOW, width), BF16),
        pltpu.VMEM((tp, 8, tok), F32),
        pltpu.VMEM((n * cap, tok), BF16),
        pltpu.VMEM((n, tok, 2 * cap), BF16),
        pltpu.VMEM((tok, width), BF16),
        pltpu.VMEM((n, cap, width), BF16),
        pltpu.VMEM((n, 8, cap), F32),
        pltpu.VMEM((n, 8, cap), F32),
        pltpu.VMEM((tp, n, cap, width), BF16),
        pltpu.VMEM((cap, hidden), BF16),
        pltpu.VMEM((n, CORES, ny, cap, width), BF16),
        pltpu.VMEM((n, ny, cap, width), BF16),
        pltpu.VMEM((ny, n, cap, width), BF16),
        pltpu.VMEM((ny, n, cap, width), BF16),
        pltpu.VMEM((n, cap, width), BF16),
        pltpu.VMEM((n, cap, width), BF16),
        pltpu.VMEM((tok, width), F32),
        pltpu.VMEM((tok, width), BF16),
        pltpu.VMEM((tok, width), BF16),
        dma((12,)),
        dma((2, 2)), dma((2, 2)),
        dma((BLOCKS,)), dma((BLOCKS,)),
        dma((BLOCKS, ny)), dma((BLOCKS, ny)),
        dma((tp,)), dma((tp,)),
        dma((n,)), dma((tp, n)), dma((n,)), dma((n,)),
        dma((n,)), dma((ny, n)), dma((ny, n)),
        dma((n,)), dma((n,)),
        dma((ny, n)), dma((ny, n)),
        dma((n,)), dma((n,)),
        dma,
    ]
    return pl.pallas_call(
        functools.partial(layer, n, tp, cap),
        out_shape=jax.ShapeDtypeStruct((tok, width), BF16),
        in_specs=[anywhere] * 12,
        out_specs=anywhere,
        scratch_shapes=scratch,
        compiler_params=pltpu.CompilerParams(
            collective_id=0, has_side_effects=True, vmem_limit_bytes=60 * 1024 * 1024
        ),
    )(
        queries, key_columns, value_columns, sink_logits[None, :], norm_gain[None, :],
        expert_ids.T, route_weights.T, out_weight, stream_in, gate_weight, up_weight,
        down_weight,
    )


def solution(mesh):
    placed = (
        P("sp", "tp"),
        P("tp", "sp"),
        P("tp", "sp"),
        P("tp"),
        P("tp", None),
        P("sp", None),
        P(),
        P("sp", None),
        P("sp", None),
        P("sp", None, "tp"),
        P("sp", None, "tp"),
        P("sp", "tp", None),
    )
    return jax.shard_map(
        functools.partial(local, mesh.shape["sp"], mesh.shape["tp"]),
        mesh=mesh, in_specs=placed, out_specs=P("sp", "tp"), check_vma=False,
    )
```

time: 98.9 us -> 91.4 us (0.924); the launches traced: 98.7 us -> 89.9 us
  Pallas kernels: 97.1 us -> 88.2 us
    pallas_call x1, Pallas kernels: 97.1 us -> 88.2 us  [local(): pl.pallas_call(functools.partial(layer, n, tp, cap), out_shape=jax.ShapeD...]
where the time goes in v1:
time: 91.4 us; the launch traced here: 89.9 us
  Pallas kernels  88.2 us (96%)
  local copies, waits for them, and re-layouts  1.67 us (2%)
    pallas_call x1, Pallas kernels, local(): pl.pallas_call(functools.partial(layer, n, tp, cap), out_shape=jax.ShapeD...  88.2 us

profile of v1, /device:TPU:8, one launch (start us, length us, event | category | flops | bytes accessed | tf_op | source)
XLA Modules:
  0.0 89.9 jit_solution(12587883946245680821)
XLA Ops:
  0.0 88.2 %shard_map.118 = bf16[256,512]{1,0:T(8,128)(2,1)} custom-call(bf16[256,512]{1,0:T(8,128)(2,1)} %q_hbm.1, bf16[256,256]{1,0:T(8,128)(2,1)} %k_hbm.1, bf16[256,256]{1,0:T(8,128)(2,1)} %v_hbm.1, f32[1,8]{1,0:T(1,128)} %bitcast.7, f32[1,2048]{1,0:T(1,128)} %bitcast.4, s32[2,256]{1,0:T(2,128)} %bitcast.5, f32[2,256]{1,0:T(2,128)} %bitcast.6, ...), custom_call_target="tpu_custom_call" | custom-call | tf_op jit(solution)/shard_map/pallas_call | solution.py:629
  88.2 1.7 %copy.14 = bf16[256,512]{1,0:T(8,128)(2,1)} copy(bf16[256,512]{1,0:T(8,128)(2,1)} %shard_map.118) | data formatting | bytes 524288

commit v2 on v1

--- a/solution.py
+++ b/solution.py
@@ -11,6 +11,7 @@
 HD = 64
 WINDOW = 128
 CORES = 2
+CHIPS_X = 2
 BLOCKS = 2
 EPSILON = 1e-06
 MASKED = -1e30
@@ -74,6 +75,57 @@
         src_ref=ref, dst_ref=ref, send_sem=sem, recv_sem=sem,
         device_id=device, device_id_type=MESH,
     ).wait_recv()
+
+
+def choose(k, table):
+    value = table[-1]
+    for at in range(len(table) - 2, -1, -1):
+        value = jnp.where(k == at, table[at], value)
+    return value
+
+
+ROLES = (
+    (
+        "F3 F5 F4 R5",
+        "F7 F1 R4 E5",
+        "R3 C5 R7 E4",
+        "F2 R1 C4 E7",
+        "E1 R2 X5 C7",
+        "E3 F6 R0 X4",
+        "E2 C3 E0 X7",
+        "R6 C1 C2 E6",
+        "X3 X1 B7 C6",
+        "B3 C0 X2 B4",
+        "X6 B1 B5 B2",
+        "B6",
+    ),
+    (
+        "R0 F4 F3 F1",
+        "R4 F2 E4 R3",
+        "R1 C4 E0 F6",
+        "E3 F7 R2 E1",
+        "C3 R6 E2 F5",
+        "X4 C1 E6 R7",
+        "X3 C6 R5 E7",
+        "E5 C7 X6 C5",
+        "C2 X1 B5 X7",
+        "C0 X5 X2 B3",
+        "B1 B6 B4 B7",
+        "B2",
+    ),
+)
+SENDS = ((4, 3, 7, 1, 6, 5, 2), (3, 5, 4, 2, 1, 6, 7))
+
+
+def plan(n):
+    if n == 8:
+        steps = [[(step[0], int(step[1:])) for step in " ".join(role).split()] for role in ROLES]
+        return SENDS, steps
+    order = [("R", 0)] + [(op, i) for i in range(1, n) for op in "FR"]
+    late = list(range(n - 1, -1, -1))
+    order += [(op, i) for i in late for op in "EC"]
+    order += [(op, i) for op in "XB" for i in late if i]
+    return [list(range(1, n))] * 2, [order] * 2
 
 
 def layer(
@@ -164,32 +216,30 @@
         @pl.when(s < n - 1)
         def _():
             for a, source in enumerate((k_ref, v_ref)):
-                send(source.at[:, pl.ds(last, WINDOW)], halo.at[a, 0],
-                     halo_send.at[a, 0], halo_recv.at[a, 0], right)
+                send(source.at[:, pl.ds(last, WINDOW)], halo.at[0, a],
+                     halo_send.at[0], halo_recv.at[0], right)
 
     def send_left():
         @pl.when(s > 0)
         def _():
             for a, source in enumerate((k_ref, v_ref)):
-                send(source.at[:, pl.ds(0, WINDOW)], halo.at[a, 1],
-                     halo_send.at[a, 1], halo_recv.at[a, 1], left)
+                send(source.at[:, pl.ds(0, WINDOW)], halo.at[1, a],
+                     halo_send.at[1], halo_recv.at[1], left)
 
     even = lax.rem(s, 2) == 0
+    odd = jnp.logical_not(even)
     pl.when(even)(send_right)
-    send_left()
-    pl.when(jnp.logical_not(even))(send_right)
+    pl.when(odd)(send_left)
     for load in loads[9:]:
         load.start()
 
     @pl.when(s == 0)
     def _():
-        for a in range(2):
-            halo[a, 0] = jnp.zeros(halo.shape[2:], BF16)
+        halo[0] = jnp.zeros(halo.shape[1:], BF16)
 
     @pl.when(s == n - 1)
     def _():
-        for a in range(2):
-            halo[a, 1] = jnp.zeros(halo.shape[2:], BF16)
+        halo[1] = jnp.zeros(halo.shape[1:], BF16)
 
     loads[2].wait()
     loads[4].wait()
@@ -234,11 +284,11 @@
 
     with scope("routing"):
         lanes = iota((tok, 128), 1).astype(F32)
+        before = (iota((tok, tok), 1) < iota((tok, tok), 0)).astype(BF16)
+
         ids = [as_column(ids_ref[k : k + 1, :].astype(F32)) for k in range(top)]
         hits = [(lanes == ids[k]).astype(F32) for k in range(top)]
-        all_hits = functools.reduce(jnp.add, hits)
-        before = (iota((tok, tok), 1) < iota((tok, tok), 0)).astype(BF16)
-        earlier = dot(before, all_hits.astype(BF16))
+        earlier = dot(before, functools.reduce(jnp.add, hits).astype(BF16))
         place = [
             jnp.sum(earlier * hits[k], axis=1, keepdims=True) + ids[k] * cap
             for k in range(top)
@@ -261,6 +311,8 @@
             return 0
 
         lax.fori_loop(0, n, picks, 0)
+    pl.when(even)(send_left)
+    pl.when(odd)(send_right)
     loads[6].wait()
     loads[7].wait()
     loads[8].wait()
@@ -273,14 +325,13 @@
 
         @pl.when(inside)
         def _():
-            for a in range(2):
-                landed(halo.at[a, b], halo_recv.at[a, b], left)
+            landed(halo.at[b], halo_recv.at[b], left)
 
         visible = (ahead * side >= 0) & (jnp.broadcast_to(inside.astype(jnp.int32), square) > 0)
         rows = pl.ds(pl.multiple_of(b * WINDOW, WINDOW), WINDOW)
         for g in range(kv_heads):
             feats = pl.ds(g * HD, HD)
-            scores = dot(query(b, g), diagonal(halo[0, b, feats, :]))
+            scores = dot(query(b, g), diagonal(halo[b, 0, feats, :]))
             weights, gap, rest = [], [], []
             for h in range(2):
                 piece = jnp.where(visible, scores[:, h * WINDOW : (h + 1) * WINDOW], MASKED)
@@ -290,7 +341,7 @@
                 gap.append(before_top - row_top)
                 rest.append(jnp.broadcast_to(sinks(g)[h] - row_top, square))
             added = dot_t(
-                jnp.concatenate(weights, axis=1), mix_matrix(halo[1, b, feats, :])
+                jnp.concatenate(weights, axis=1), mix_matrix(halo[b, 1, feats, :])
             )
             old = own_o[b, g]
             shrink = jnp.exp(jnp.where(low_lanes, gap[0], gap[1]))
@@ -307,7 +358,7 @@
 
     def swap(b):
         project(b, other)
-        send(part.at[b, other], part_in.at[b], ps_send.at[b], ps_recv.at[b], partner)
+        send(part.at[b, other], part_in.at[b], ps_send, ps_recv.at[b], partner)
         project(b, c)
 
     def across(b):
@@ -317,13 +368,13 @@
             part_sum[b, dy] = (
                 part[b, c, yy].astype(F32) + part_in[b, yy].astype(F32)
             ).astype(BF16)
-            send(part_sum.at[b, dy], part_y.at[b, dy], py_send.at[b, dy], py_recv.at[b, dy],
+            send(part_sum.at[b, dy], part_y.at[b, dy], py_send, py_recv.at[b, dy - 1],
                  at_tp(yy * CORES + c))
 
     def settle(b):
         attn = part[b, c, y].astype(F32) + part_in[b, y].astype(F32)
         for dy in range(1, ny):
-            landed(part_y.at[b, dy], py_recv.at[b, dy], at_tp(from_y(dy) * CORES + c))
+            landed(part_y.at[b, dy], py_recv.at[b, dy - 1], at_tp(from_y(dy) * CORES + c))
             attn = attn + part_y[b, dy].astype(F32)
         rows = pl.ds(pl.multiple_of(b * WINDOW, WINDOW), WINDOW)
         res = (stream[rows, :].astype(F32) + attn.astype(BF16).astype(F32)).astype(BF16)
@@ -353,43 +404,46 @@
     with scope("settle1"):
         settle(second)
     for dt in range(1, tp):
-        send(squares.at[0], squares.at[dt], sq_send.at[dt], sq_recv.at[dt],
+        send(squares.at[0], squares.at[dt], sq_send, sq_recv.at[dt - 1],
              at_tp(lax.rem(t + dt, tp)))
 
-    def lane(k):
-        return jnp.where(k < 2, k, jnp.where(k < 2 + n // 2, k - 2 + n // 2, k - n // 2))
-
-    def rows_of(i):
-        chosen = pick[pl.ds(pl.multiple_of(i * cap, cap), cap), :]
-        return dot(chosen, rows_out[...]).astype(BF16)
-
-    def forward(k):
-        i = lane(k)
-
+    sends, steps = plan(n)
+    place_z = s // CHIPS_X
+    outer = (place_z == 0) | (place_z == n // CHIPS_X - 1)
+
+    def by_role(k, tables):
+        return jnp.where(outer, choose(k, tables[1]), choose(k, tables[0]))
+
+
+    def chosen(i, source):
+        rows = pick[pl.ds(pl.multiple_of(i * cap, cap), cap), :]
+        return dot(rows, source[...]).astype(BF16)
+
+    def forward(i):
         @pl.when(i > 0)
         def _():
             landed(xb.at[t, i], x_recv.at[t, i], right)
 
         for dy in range(1, ny):
-            send(xb.at[t, i], xb.at[t, i], fy_send.at[dy, i], x_recv.at[t, i],
+            send(xb.at[t, i], xb.at[t, i], fy_send, x_recv.at[t, i],
                  at_tp(peer_y(dy) * CORES + c))
-        send(xb.at[t, i], xb.at[t, i], fc_send.at[i], x_recv.at[t, i], partner)
+        send(xb.at[t, i], xb.at[t, i], fc_send, x_recv.at[t, i], partner)
 
     def dispatch(k, _):
-        i = lane(k)
-        slots[i] = rows_of(i)
-        send(slots.at[i], xb.at[t, i], d_send.at[i], x_recv.at[t, i], at_sp(pair(i)))
+        i = by_role(k, sends)
+        slots[i] = chosen(i, rows_out)
+        send(slots.at[i], xb.at[t, i], d_send, x_recv.at[t, i], at_sp(pair(i)))
         return 0
 
     with scope("dispatch"):
-        xb[t, 0] = rows_of(0)
+        xb[t, 0] = chosen(0, rows_out)
         forward(0)
-        lax.fori_loop(1, n, dispatch, 0)
+        dispatch(0, 0)
 
     with scope("scales"):
         square_sum = squares[0]
         for dt in range(1, tp):
-            landed(squares.at[dt], sq_recv.at[dt], at_tp(lax.rem(t + tp - dt, tp)))
+            landed(squares.at[dt], sq_recv.at[dt - 1], at_tp(lax.rem(t + tp - dt, tp)))
             square_sum = square_sum + squares[dt]
         inverse = lax.rsqrt(square_sum / (tp * width) + EPSILON)
         high = inverse.astype(BF16).astype(F32)
@@ -406,29 +460,25 @@
                 scale_in[0] = piece
             else:
                 scale_out[i] = piece
-                send(scale_out.at[i], scale_in.at[i], sc_send.at[i], sc_recv.at[i],
+                send(scale_out.at[i], scale_in.at[i], sc_send, sc_recv.at[i],
                      at_sp(pair(i)))
+
+    with scope("late"):
+        lax.fori_loop(1, n - 1, dispatch, 0)
 
     with scope("weights"):
         for load in loads[9:]:
             load.wait()
 
-    def turn(j):
-        return jnp.where(
-            j < n // 2, j + n // 2, jnp.where(j < n - 2, j + 2 - n // 2, n - 1 - j)
-        )
-
-    def relay(k):
-        i = lane(k)
+    def relay(i):
         for dy in range(1, ny):
             j = from_y(dy) * CORES + c
             landed(xb.at[j, i], x_recv.at[j, i], at_tp(j))
-            send(xb.at[j, i], xb.at[j, i], f2_send.at[dy, i], x_recv.at[j, i], partner)
+            send(xb.at[j, i], xb.at[j, i], f2_send, x_recv.at[j, i], partner)
 
     tile = min(hidden, 256)
 
-    def expert(k):
-        i = turn(k)
+    def expert(i):
         for yy in range(ny):
             j = yy * CORES + other
             landed(xb.at[j, i], x_recv.at[j, i], partner)
@@ -448,114 +498,82 @@
             po[i, j % CORES, j // CORES] = dot(
                 hid[...], down[:, j * width : (j + 1) * width]
             ).astype(BF16)
-        send(po.at[i, other], po_in.at[i], po_send.at[i], po_recv.at[i], partner)
-
-    def chip_add(k):
-        i = turn(k)
+        send(po.at[i, other], po_in.at[i], po_send, po_recv.at[i], partner)
+
+    def chip_add(i):
         landed(po_in.at[i], po_recv.at[i], partner)
         for dy in range(1, ny):
             yy = peer_y(dy)
             chip_sum[dy, i] = (po[i, c, yy].astype(F32) + po_in[i, yy].astype(F32)).astype(BF16)
-            send(chip_sum.at[dy, i], sum_y.at[dy, i], y_send.at[dy, i], y_recv.at[dy, i],
+            send(chip_sum.at[dy, i], sum_y.at[dy, i], y_send, y_recv.at[dy - 1, i],
                  at_tp(yy * CORES + c))
 
     def whole(i):
         total = po[i, c, y].astype(F32) + po_in[i, y].astype(F32)
         for dy in range(1, ny):
-            landed(sum_y.at[dy, i], y_recv.at[dy, i], at_tp(from_y(dy) * CORES + c))
+            landed(sum_y.at[dy, i], y_recv.at[dy - 1, i], at_tp(from_y(dy) * CORES + c))
             total = total + sum_y[dy, i].astype(F32)
         return total.astype(BF16)
 
-    def finish(k):
-        i = turn(k)
+    def finish(i):
         final[i] = whole(i)
-        send(final.at[i], back.at[i], r_send.at[i], r_recv.at[i], at_sp(pair(i)))
-
-    stages = (
-        (0, n, forward), (5, n, chip_add), (1, n, relay), (4, n, expert), (6, n - 1, finish),
-    )
-
-    def step(k, _):
-        for lag, count, stage in stages:
-            first_step = max(lag, 1)
-
-            @pl.when((k >= first_step) & (k - lag < count))
-            def _(stage=stage, lag=lag):
-                with scope(stage.__name__):
-                    stage(k - lag)
-        return 0
-
-    lax.fori_loop(1, n + 5, step, 0)
+        send(final.at[i], back.at[i], r_send, r_recv.at[i], at_sp(pair(i)))
 
     def blend(i):
         rows = back[i]
         return dot(mixer[i], jnp.concatenate([rows, rows], axis=0))
 
-    def returned(i, _):
+    def returned(i):
         landed(back.at[i], r_recv.at[i], right)
         mixed[...] += blend(i)
+
+    mixed[...] = residual[...].astype(F32)
+    stages = dict(
+        F=forward, R=relay, E=expert, C=chip_add, X=finish, B=returned
+    )
+    codes = [
+        [list(stages).index(op) * n + i for op, i in order] for order in steps
+    ]
+
+    def step(k, _):
+        code = by_role(k, codes)
+        for at, (name, stage) in enumerate(stages.items()):
+            @pl.when((code >= at * n) & (code < (at + 1) * n))
+            def _(stage=stage, name=name, at=at):
+                with scope(name):
+                    stage(code - at * n)
         return 0
 
-    with scope("returned"):
-        mixed[...] = residual[...].astype(F32)
-        lax.fori_loop(2, n, returned, 0)
+    lax.fori_loop(0, len(codes[0]), step, 0)
 
     with scope("drain"):
         @pl.when(s < n - 1)
         def _():
-            for a in range(2):
-                sent(halo.at[a, 0], halo_send.at[a, 0], right)
+            sent(halo.at[0], halo_send.at[0], right)
 
         @pl.when(s > 0)
         def _():
-            for a in range(2):
-                sent(halo.at[a, 1], halo_send.at[a, 1], left)
-
-        for b in range(BLOCKS):
-            sent(part_in.at[b], ps_send.at[b], partner)
-            for dy in range(1, ny):
-                sent(part_sum.at[b, dy], py_send.at[b, dy], partner)
-        for dt in range(1, tp):
-            sent(squares.at[0], sq_send.at[dt], partner)
-
-        def drain(i, _):
-            @pl.when(i > 0)
-            def _():
-                sent(slots.at[i], d_send.at[i], right)
-                sent(scale_out.at[i], sc_send.at[i], right)
-
-            @pl.when(i > 1)
-            def _():
-                sent(final.at[i], r_send.at[i], right)
-
-            sent(final.at[i], fc_send.at[i], partner)
-            sent(po_in.at[i], po_send.at[i], partner)
-            for dy in range(1, ny):
-                sent(final.at[i], fy_send.at[dy, i], partner)
-                sent(final.at[i], f2_send.at[dy, i], partner)
-            return 0
-
-        lax.fori_loop(0, n, drain, 0)
+            sent(halo.at[1], halo_send.at[1], left)
+
+        others = pl.ds(1, ny - 1)
+        sent(part_in, ps_send, partner)
+        sent(part_sum.at[:, others], py_send, partner)
+        sent(squares.at[pl.ds(1, tp - 1)], sq_send, partner)
+        sent(slots.at[pl.ds(1, n - 1)], d_send, right)
+        sent(scale_out.at[pl.ds(1, n - 1)], sc_send, right)
+        sent(final, fc_send, partner)
+        sent(po_in, po_send, partner)
+        for sem in (fy_send, f2_send):
+            sent(chip_sum.at[others], sem, partner)
 
     with scope("own"):
         back[0] = whole(0)
-        mixed[...] += blend(0)
-
-    with scope("near"):
-        landed(back.at[1], r_recv.at[1], right)
-        out[...] = (mixed[...] + blend(1)).astype(BF16)
+        out[...] = (mixed[...] + blend(0)).astype(BF16)
     put = pltpu.make_async_copy(out, out_hbm, out_sem)
     put.start()
-    sent(final.at[1], r_send.at[1], right)
-
-    def drain_y(i, _):
-        for dy in range(1, ny):
-            sent(final.at[i], y_send.at[dy, i], partner)
-        return 0
-
-    with scope("exit"):
-        lax.fori_loop(0, n, drain_y, 0)
-        put.wait()
+    sent(chip_sum.at[others], y_send, partner)
+    sent(final.at[pl.ds(1, n - 1)], r_send, right)
+    put.wait()
 
 
 def local(
@@ -615,15 +633,15 @@
         pltpu.VMEM((tok, width), BF16),
         pltpu.VMEM((tok, width), BF16),
         dma((12,)),
-        dma((2, 2)), dma((2, 2)),
-        dma((BLOCKS,)), dma((BLOCKS,)),
-        dma((BLOCKS, ny)), dma((BLOCKS, ny)),
-        dma((tp,)), dma((tp,)),
-        dma((n,)), dma((tp, n)), dma((n,)), dma((n,)),
-        dma((n,)), dma((ny, n)), dma((ny, n)),
-        dma((n,)), dma((n,)),
-        dma((ny, n)), dma((ny, n)),
-        dma((n,)), dma((n,)),
+        dma((2,)), dma((2,)),
+        dma, dma((BLOCKS,)),
+        dma, dma((BLOCKS, ny - 1)),
+        dma, dma((tp - 1,)),
+        dma, dma((tp, n)), dma, dma((n,)),
+        dma, dma, dma,
+        dma, dma((n,)),
+        dma, dma((ny - 1, n)),
+        dma, dma((n,)),
         dma,
     ]
     return pl.pallas_call(

time: 91.4 us -> 85.9 us (0.940)
  the two profiles are of different devices: /device:TPU:8 before, /device:TPU:10 now
where the time goes in v2:
time: 85.9 us; the launch traced here: 85.8 us
  Pallas kernels  84.1 us (98%)
  local copies, waits for them, and re-layouts  1.67 us (2%)
    pallas_call x1, Pallas kernels, local(): pl.pallas_call(functools.partial(layer, n, tp, cap), out_shape=jax.ShapeD...  84.1 us

profile of v2, /device:TPU:10, one launch (start us, length us, event | category | flops | bytes accessed | tf_op | source)
XLA Modules:
  0.0 85.8 jit_solution(12316755020727377294)
XLA Ops:
  0.0 84.1 %shard_map.118 = bf16[256,512]{1,0:T(8,128)(2,1)} custom-call(bf16[256,512]{1,0:T(8,128)(2,1)} %q_hbm.1, bf16[256,256]{1,0:T(8,128)(2,1)} %k_hbm.1, bf16[256,256]{1,0:T(8,128)(2,1)} %v_hbm.1, f32[1,8]{1,0:T(1,128)} %bitcast.7, f32[1,2048]{1,0:T(1,128)} %bitcast.4, s32[2,256]{1,0:T(2,128)} %bitcast.5, f32[2,256]{1,0:T(2,128)} %bitcast.6, ...), custom_call_target="tpu_custom_call" | custom-call | tf_op jit(solution)/shard_map/pallas_call | solution.py:647
  84.1 1.7 %copy.14 = bf16[256,512]{1,0:T(8,128)(2,1)} copy(bf16[256,512]{1,0:T(8,128)(2,1)} %shard_map.118) | data formatting | bytes 524288

commit v3 on v2

--- a/solution.py
+++ b/solution.py
@@ -13,6 +13,9 @@
 CORES = 2
 CHIPS_X = 2
 BLOCKS = 2
+BASE = 256
+DIGITS = 3
+EARLY = (3, 3)
 EPSILON = 1e-06
 MASKED = -1e30
 MESH = pl.DeviceIdType.MESH
@@ -86,35 +89,35 @@
 
 ROLES = (
     (
-        "F3 F5 F4 R5",
-        "F7 F1 R4 E5",
-        "R3 C5 R7 E4",
-        "F2 R1 C4 E7",
-        "E1 R2 X5 C7",
-        "E3 F6 R0 X4",
-        "E2 C3 E0 X7",
-        "R6 C1 C2 E6",
-        "X3 X1 B7 C6",
-        "B3 C0 X2 B4",
-        "X6 B1 B5 B2",
-        "B6",
+        "F1 F4 F6 F3",
+        "R4 F5 R1 E4",
+        "C4 R3 E1 F2",
+        "R6 E3 F7 E6",
+        "R5 X4 C6 R0",
+        "E5 C5 R2 X6",
+        "C3 R7 E2 X5",
+        "C1 E7 C2 E0",
+        "X1 X3 C7 X2",
+        "X7 B3 C0 B1",
+        "B4 B5 B6 B2",
+        "B7",
     ),
     (
-        "R0 F4 F3 F1",
-        "R4 F2 E4 R3",
-        "R1 C4 E0 F6",
-        "E3 F7 R2 E1",
-        "C3 R6 E2 F5",
-        "X4 C1 E6 R7",
-        "X3 C6 R5 E7",
-        "E5 C7 X6 C5",
-        "C2 X1 B5 X7",
-        "C0 X5 X2 B3",
-        "B1 B6 B4 B7",
-        "B2",
+        "F6 F1 R6 F3",
+        "E6 R0 F2 R3",
+        "R1 C6 E0 R2",
+        "F7 E1 F4 E3",
+        "C1 R7 X6 F5",
+        "E7 R4 C7 E4",
+        "C3 R5 E2 C4",
+        "X7 E5 X3 C5",
+        "C2 X4 X1 B6",
+        "X5 B7 C0 X2",
+        "B5 B3 B1 B2",
+        "B4",
     ),
 )
-SENDS = ((4, 3, 7, 1, 6, 5, 2), (3, 5, 4, 2, 1, 6, 7))
+SENDS = ((1, 6, 2, 4, 7, 3, 5), (6, 1, 4, 3, 5, 2, 7))
 
 
 def plan(n):
@@ -391,10 +394,10 @@
         attend(first)
     with scope("swap0"):
         swap(first)
+    with scope("across0"):
+        across(first)
     with scope("attend1"):
         attend(second)
-    with scope("across0"):
-        across(first)
     with scope("swap1"):
         swap(second)
     with scope("across1"):
@@ -411,8 +414,21 @@
     place_z = s // CHIPS_X
     outer = (place_z == 0) | (place_z == n // CHIPS_X - 1)
 
-    def by_role(k, tables):
-        return jnp.where(outer, choose(k, tables[1]), choose(k, tables[0]))
+    def packed(tables):
+        tables = [table + [0] * (-len(table) % DIGITS) for table in map(list, tables)]
+        words = [
+            [sum(d * BASE**p for p, d in enumerate(table[at : at + DIGITS]))
+             for at in range(0, len(table), DIGITS)]
+            for table in tables
+        ]
+        return [jnp.where(outer, b, a) for a, b in zip(*words)]
+
+    def unpacked(k, words):
+        word = choose(k // DIGITS, words)
+        return choose(k % DIGITS, [word // BASE**p % BASE for p in range(DIGITS)])
+
+    send_words = packed(sends)
+    early = jnp.where(outer, EARLY[1], EARLY[0])
 
 
     def chosen(i, source):
@@ -430,7 +446,7 @@
         send(xb.at[t, i], xb.at[t, i], fc_send, x_recv.at[t, i], partner)
 
     def dispatch(k, _):
-        i = by_role(k, sends)
+        i = unpacked(k, send_words)
         slots[i] = chosen(i, rows_out)
         send(slots.at[i], xb.at[t, i], d_send, x_recv.at[t, i], at_sp(pair(i)))
         return 0
@@ -438,7 +454,7 @@
     with scope("dispatch"):
         xb[t, 0] = chosen(0, rows_out)
         forward(0)
-        dispatch(0, 0)
+        lax.fori_loop(0, early, dispatch, 0)
 
     with scope("scales"):
         square_sum = squares[0]
@@ -464,7 +480,7 @@
                      at_sp(pair(i)))
 
     with scope("late"):
-        lax.fori_loop(1, n - 1, dispatch, 0)
+        lax.fori_loop(early, n - 1, dispatch, 0)
 
     with scope("weights"):
         for load in loads[9:]:
@@ -494,11 +510,16 @@
             gate_pre = dot(rows, gate[:, cols]) * scale
             upward = dot(rows, up[:, cols]) * scale
             hid[:, cols] = (gate_pre / (1.0 + jnp.exp(-gate_pre)) * upward).astype(BF16)
-        for j in range(tp):
-            po[i, j % CORES, j // CORES] = dot(
-                hid[...], down[:, j * width : (j + 1) * width]
-            ).astype(BF16)
+        activated = hid[...]
+
+        def lower(core):
+            for yy in range(ny):
+                start = pl.multiple_of((yy * CORES + core) * width, 128)
+                po[i, core, yy] = dot(activated, down[:, pl.ds(start, width)]).astype(BF16)
+
+        lower(other)
         send(po.at[i, other], po_in.at[i], po_send, po_recv.at[i], partner)
+        lower(c)
 
     def chip_add(i):
         landed(po_in.at[i], po_recv.at[i], partner)
@@ -535,8 +556,10 @@
         [list(stages).index(op) * n + i for op, i in order] for order in steps
     ]
 
+    code_words = packed(codes)
+
     def step(k, _):
-        code = by_role(k, codes)
+        code = unpacked(k, code_words)
         for at, (name, stage) in enumerate(stages.items()):
             @pl.when((code >= at * n) & (code < (at + 1) * n))
             def _(stage=stage, name=name, at=at):

time: 85.9 us -> 76.7 us (0.89)
  the two profiles are of different devices: /device:TPU:10 before, /device:TPU:8 now
where the time goes in v3:
time: 76.7 us; the launch traced here: 76.1 us
  Pallas kernels  74.5 us (97%)
  local copies, waits for them, and re-layouts  1.67 us (2%)
    pallas_call x1, Pallas kernels, local(): pl.pallas_call(functools.partial(layer, n, tp, cap), out_shape=jax.ShapeD...  74.5 us
    unnamed x1, local copies, waits for them, and re-layouts  1.67 us

profile of v3, /device:TPU:8, one launch (start us, length us, event | category | flops | bytes accessed | tf_op | source)
XLA Modules:
  0.0 76.1 jit_solution(2195212228554924846)
XLA Ops:
  0.0 74.5 %shard_map.118 = bf16[256,512]{1,0:T(8,128)(2,1)} custom-call(bf16[256,512]{1,0:T(8,128)(2,1)} %q_hbm.1, bf16[256,256]{1,0:T(8,128)(2,1)} %k_hbm.1, bf16[256,256]{1,0:T(8,128)(2,1)} %v_hbm.1, f32[1,8]{1,0:T(1,128)} %bitcast.7, f32[1,2048]{1,0:T(1,128)} %bitcast.4, s32[2,256]{1,0:T(2,128)} %bitcast.5, f32[2,256]{1,0:T(2,128)} %bitcast.6, ...), custom_call_target="tpu_custom_call" | custom-call | tf_op jit(solution)/shard_map/pallas_call | solution.py:670
  74.5 1.7 %copy.14 = bf16[256,512]{1,0:T(8,128)(2,1)} copy(bf16[256,512]{1,0:T(8,128)(2,1)} %shard_map.118) | data formatting | bytes 524288

commit v4 on v3

--- a/solution.py
+++ b/solution.py
@@ -93,8 +93,8 @@
         "R4 F5 R1 E4",
         "C4 R3 E1 F2",
         "R6 E3 F7 E6",
-        "R5 X4 C6 R0",
-        "E5 C5 R2 X6",
+        "R5 X4 C6 E5",
+        "C5 R0 R2 X6",
         "C3 R7 E2 X5",
         "C1 E7 C2 E0",
         "X1 X3 C7 X2",
@@ -117,7 +117,7 @@
         "B4",
     ),
 )
-SENDS = ((1, 6, 2, 4, 7, 3, 5), (6, 1, 4, 3, 5, 2, 7))
+SENDS = ((1, 6, 2, 4, 7, 3, 5), (6, 1, 4, 3, 5, 7, 2))
 
 
 def plan(n):
@@ -220,14 +220,14 @@
         def _():
             for a, source in enumerate((k_ref, v_ref)):
                 send(source.at[:, pl.ds(last, WINDOW)], halo.at[0, a],
-                     halo_send.at[0], halo_recv.at[0], right)
+                     halo_send.at[0], halo_recv.at[0, a], right)
 
     def send_left():
         @pl.when(s > 0)
         def _():
             for a, source in enumerate((k_ref, v_ref)):
                 send(source.at[:, pl.ds(0, WINDOW)], halo.at[1, a],
-                     halo_send.at[1], halo_recv.at[1], left)
+                     halo_send.at[1], halo_recv.at[1, a], left)
 
     even = lax.rem(s, 2) == 0
     odd = jnp.logical_not(even)
@@ -326,12 +326,15 @@
         edge = s + b * n
         inside = jnp.logical_and(edge > 0, edge < 2 * n - 1)
 
-        @pl.when(inside)
-        def _():
-            landed(halo.at[b], halo_recv.at[b], left)
+        def arrived(a):
+            @pl.when(inside)
+            def _():
+                landed(halo.at[b, a], halo_recv.at[b, a], left)
 
         visible = (ahead * side >= 0) & (jnp.broadcast_to(inside.astype(jnp.int32), square) > 0)
         rows = pl.ds(pl.multiple_of(b * WINDOW, WINDOW), WINDOW)
+        arrived(0)
+        held = []
         for g in range(kv_heads):
             feats = pl.ds(g * HD, HD)
             scores = dot(query(b, g), diagonal(halo[b, 0, feats, :]))
@@ -343,31 +346,34 @@
                 weights.append(jnp.exp(piece - row_top).astype(BF16))
                 gap.append(before_top - row_top)
                 rest.append(jnp.broadcast_to(sinks(g)[h] - row_top, square))
-            added = dot_t(
-                jnp.concatenate(weights, axis=1), mix_matrix(halo[b, 1, feats, :])
-            )
-            old = own_o[b, g]
             shrink = jnp.exp(jnp.where(low_lanes, gap[0], gap[1]))
             total = jnp.exp(jnp.where(low_lanes, rest[0], rest[1]))
+            held.append((jnp.concatenate(weights, axis=1), shrink, total))
+        arrived(1)
+        for g, (weights, shrink, total) in enumerate(held):
+            feats = pl.ds(g * HD, HD)
+            added = dot_t(weights, mix_matrix(halo[b, 1, feats, :]))
+            old = own_o[b, g]
             total = total + old[:, 2 * HD :] * shrink + added[:, 2 * HD :]
             value = old[:, : 2 * HD] * shrink + added[:, : 2 * HD]
             head[rows, pl.ds(g * 2 * HD, 2 * HD)] = (value / total).astype(BF16)
 
-    def project(b, core):
+    def project(b, core, yy):
         mine = head[pl.ds(pl.multiple_of(b * WINDOW, WINDOW), WINDOW), :]
-        for yy in range(ny):
-            start = pl.multiple_of((yy * CORES + core) * width, 128)
-            part[b, core, yy] = dot(mine, ow[:, pl.ds(start, width)]).astype(BF16)
+        start = pl.multiple_of((yy * CORES + core) * width, 128)
+        part[b, core, yy] = dot(mine, ow[:, pl.ds(start, width)]).astype(BF16)
 
     def swap(b):
-        project(b, other)
-        send(part.at[b, other], part_in.at[b], ps_send, ps_recv.at[b], partner)
-        project(b, c)
+        for dy in list(range(1, ny)) + [0]:
+            yy = peer_y(dy)
+            project(b, other, yy)
+            send(part.at[b, other, yy], part_in.at[b, yy], ps_send, ps_recv.at[b, yy], partner)
+            project(b, c, yy)
 
     def across(b):
-        landed(part_in.at[b], ps_recv.at[b], partner)
         for dy in range(1, ny):
             yy = peer_y(dy)
+            landed(part_in.at[b, yy], ps_recv.at[b, yy], partner)
             part_sum[b, dy] = (
                 part[b, c, yy].astype(F32) + part_in[b, yy].astype(F32)
             ).astype(BF16)
@@ -375,6 +381,7 @@
                  at_tp(yy * CORES + c))
 
     def settle(b):
+        landed(part_in.at[b, y], ps_recv.at[b, y], partner)
         attn = part[b, c, y].astype(F32) + part_in[b, y].astype(F32)
         for dy in range(1, ny):
             landed(part_y.at[b, dy], py_recv.at[b, dy - 1], at_tp(from_y(dy) * CORES + c))
@@ -656,8 +663,8 @@
         pltpu.VMEM((tok, width), BF16),
         pltpu.VMEM((tok, width), BF16),
         dma((12,)),
-        dma((2,)), dma((2,)),
-        dma, dma((BLOCKS,)),
+        dma((2,)), dma((2, 2)),
+        dma, dma((BLOCKS, ny)),
         dma, dma((BLOCKS, ny - 1)),
         dma, dma((tp - 1,)),
         dma, dma((tp, n)), dma, dma((n,)),

time: 76.7 us -> 76 us (level)
  no operation moved by 1% of the time
where the time goes in v4:
time: 76 us; the launch traced here: 75.7 us
  Pallas kernels  74 us (97%)
  local copies, waits for them, and re-layouts  1.67 us (2%)
    pallas_call x1, Pallas kernels, local(): pl.pallas_call(functools.partial(layer, n, tp, cap), out_shape=jax.ShapeD...  74 us
    unnamed x1, local copies, waits for them, and re-layouts  1.67 us

profile of v4, /device:TPU:8, one launch (start us, length us, event | category | flops | bytes accessed | tf_op | source)
XLA Modules:
  0.0 75.7 jit_solution(16129268128665155622)
XLA Ops:
  0.0 74.0 %shard_map.118 = bf16[256,512]{1,0:T(8,128)(2,1)} custom-call(bf16[256,512]{1,0:T(8,128)(2,1)} %q_hbm.1, bf16[256,256]{1,0:T(8,128)(2,1)} %k_hbm.1, bf16[256,256]{1,0:T(8,128)(2,1)} %v_hbm.1, f32[1,8]{1,0:T(1,128)} %bitcast.7, f32[1,2048]{1,0:T(1,128)} %bitcast.4, s32[2,256]{1,0:T(2,128)} %bitcast.5, f32[2,256]{1,0:T(2,128)} %bitcast.6, ...), custom_call_target="tpu_custom_call" | custom-call | tf_op jit(solution)/shard_map/pallas_call | solution.py:677
  74.0 1.7 %copy.14 = bf16[256,512]{1,0:T(8,128)(2,1)} copy(bf16[256,512]{1,0:T(8,128)(2,1)} %shard_map.118) | data formatting | bytes 524288
